TPU v7x, 32 devices: a whole 2x2x4 slice. The times are simulated.
32 devices in a mesh: fs: 16 (over z, y, x), tp: 2 (over core).
Axes of the slice: x: 2, y: 2, z: 4, core: 2. Of those that a mesh axis runs over, the one named last changes fastest.
Arguments:
- tokens: bfloat16 [5120, 2048], P('fs'), may hold values from -6 to 6
- w_gate: bfloat16 [2048, 5632], P('fs', 'tp'), may hold values from -0.125 to 0.125
- w_up: bfloat16 [2048, 5632], P('fs', 'tp'), may hold values from -0.125 to 0.125
- w_down: bfloat16 [5632, 2048], P('tp', 'fs'), may hold values from -0.078125 to 0.078125
- w_mix_in: bfloat16 [2048, 1024], P('fs', 'tp'), may hold values from -0.125 to 0.125
- w_mix_out: bfloat16 [1024, 2048], P('tp', 'fs'), may hold values from -0.1875 to 0.1875
- pool_w: bfloat16 [8, 128, 128], P('tp'), may hold values from -0.5 to 0.5
- pool_scale: bfloat16 [1024], P('tp'), may hold values from 0.099609375 to 1.8984375
- norm_gains: float32 [6, 2048], replicated, may hold values from 0.1 to 1.9
Outputs:
- layer_out: bfloat16 [5120, 2048], P(('fs', 'tp'))
All inputs are finite; a program needn't handle non-finite values.
Results may differ from a plain program's by a relative error of at most 0.018.
Values may be sent and summed in bfloat16 or wider, within the bound.
A program may use at most 128 MiB of HBM per device.

v0:
```python
import jax
import jax.numpy as jnp
from jax import lax
from jax.sharding import PartitionSpec as P

LEN = 64


def rms_scale(values, gain):
    return values * lax.rsqrt(jnp.mean(values * values, axis=-1, keepdims=True) + 1e-06) * gain


def reduce_rows(left_rows, right_matrix):
    return lax.psum_scatter(
        jnp.dot(left_rows, right_matrix, preferred_element_type=jnp.float32).astype(jnp.bfloat16),
        "tp",
        scatter_dimension=0,
        tiled=True,
    ).astype(jnp.float32)


def gather_rows(normed, project):
    return project(lax.all_gather(normed, "tp", axis=0, tiled=True), jnp.int32(0))


def body(tokens, w_gate, w_up, w_down, w_mix_in, w_mix_out, pool_w, pool_scale, norm_gains):
    tp_size = lax.axis_size("tp")
    rows_all = tokens.shape[0]
    own_rows = rows_all // tp_size
    stream = tokens.astype(jnp.float32)
    normed = rms_scale(stream, norm_gains[0]).astype(jnp.bfloat16)
    down_full, mix_in_full, mix_out_full = (
        lax.all_gather(w_down, "fs", axis=1, tiled=True),
        lax.all_gather(w_mix_in, "fs", axis=0, tiled=True),
        lax.all_gather(w_mix_out, "fs", axis=1, tiled=True),
    )
    gate_full, up_full = (
        lax.all_gather(w_gate, "fs", axis=0, tiled=True),
        lax.all_gather(w_up, "fs", axis=0, tiled=True),
    )
    gate_first = jnp.dot(normed, gate_full, preferred_element_type=jnp.float32)
    up_first = jnp.dot(normed, up_full, preferred_element_type=jnp.float32)
    hidden = (jax.nn.silu(gate_first) * up_first).astype(jnp.bfloat16)
    stream_own = lax.dynamic_slice_in_dim(stream, lax.axis_index("tp") * own_rows, own_rows, 0)
    stream_own = stream_own + 0.5 * rms_scale(reduce_rows(hidden, down_full), norm_gains[1])
    normed = rms_scale(stream_own, norm_gains[2]).astype(jnp.bfloat16)

    def project_pool(part_rows, offset):
        return jnp.dot(part_rows, mix_in_full, preferred_element_type=jnp.float32).astype(
            jnp.bfloat16
        )

    pooled_in = gather_rows(normed, project_pool)
    groups_here = pool_w.shape[0]
    group_dim = pool_w.shape[1]
    values = pooled_in.astype(jnp.float32).reshape(rows_all // LEN, LEN, groups_here, group_dim)
    totals = jnp.cumsum(values, axis=1)
    position = jnp.arange(1, LEN + 1).astype(jnp.float32)[None, :, None, None]
    window_ids = (lax.axis_index("tp") * groups_here + jnp.arange(groups_here)) % 4
    average = jnp.zeros_like(values)
    for window_slot in range(4):
        window = 2 ** (1 + window_slot)
        lagged = jnp.pad(totals, ((0, 0), (window, 0), (0, 0), (0, 0)))[:, :LEN]
        candidate = (totals - lagged) / jnp.minimum(position, float(window))
        average = jnp.where((window_ids == window_slot)[None, None, :, None], candidate, average)
    deviation = (average - values).astype(jnp.bfloat16)
    regrouped = jnp.einsum("btgi,gio->btgo", deviation, pool_w, preferred_element_type=jnp.float32)
    regrouped = (
        regrouped.reshape(rows_all, groups_here * group_dim) * pool_scale.astype(jnp.float32)
    ).astype(jnp.bfloat16)
    stream_own = stream_own + rms_scale(reduce_rows(regrouped, mix_out_full), norm_gains[3])
    normed = rms_scale(stream_own, norm_gains[4]).astype(jnp.bfloat16)

    def project_ffn(part_rows, offset):
        gate_part = jnp.dot(part_rows, gate_full, preferred_element_type=jnp.float32)
        up_part = jnp.dot(part_rows, up_full, preferred_element_type=jnp.float32)
        return (jax.nn.silu(gate_part) * up_part).astype(jnp.bfloat16)

    hidden = gather_rows(normed, project_ffn)
    stream_own = stream_own + 0.5 * rms_scale(reduce_rows(hidden, down_full), norm_gains[5])
    return stream_own.astype(jnp.bfloat16)


def solution(mesh):
    in_specs = (
        P("fs", None),
        P("fs", "tp"),
        P("fs", "tp"),
        P("tp", "fs"),
        P("fs", "tp"),
        P("tp", "fs"),
        P("tp", None, None),
        P("tp"),
        P(),
    )
    out_specs = P(("fs", "tp"), None)
    return jax.shard_map(body, mesh=mesh, in_specs=in_specs, out_specs=out_specs, check_vma=False)
```

profile of v0, /device:TPU:0, one launch (start us, length us, event | category | flops | bytes accessed | tf_op | source)
XLA Modules:
  0.0 719.4 jit_solution(5918043827711091280)
XLA Ops:
  6.5 0.7 all-gather.8.cloned.1.call-update
  7.3 0.0 all-gather.10.cloned.1.call-start
  7.3 0.7 all-gather.10.cloned.1.call-update
  8.0 0.0 all-gather.12.cloned.1.call-start
  8.1 0.7 all-gather.12.cloned.1.call-update
  8.8 0.0 reduce-scatter.4.cloned.1.call-start
  8.8 0.4 multiply_reduce_fusion
  9.2 145.0 %all-gather.8.cloned.1.call-done = bf16[2048,2816]{1,0:T(8,128)(2,1)} async-done(((bf16[128,2816]{1,0:T(8,128)(2,1)}), bf16[2048,2816]{1,0:T(8,128)(2,1)}) %all-gather.8.cloned.1.call-update) | async-done | bytes 11534352 | tf_op jit(solution)/shard_map/all_gather | solution.py:38
  154.3 8.7 %fusion.23 = f32[320,2816]{1,0:T(8,128)} fusion(bf16[2048,2816]{1,0:T(8,128)(2,1)} %all-gather.8.cloned.1.call-done, f32[2048]{0:T(1024)S(1)} %bitcast.40, f32[320]{0:T(512)S(1)} %add_rsqrt_fusion, bf16[320,2048]{1,0:T(8,128)(2,1)S(1)} %copy-done.3), kind=kOutput, calls=%fused_computation.50 | convolution fusion | flops 3693608960 | bytes 16459008 | tf_op jit(solution)/shard_map/dot_general | solution.py:41
  163.0 133.7 %all-gather.10.cloned.1.call-done = bf16[2048,2816]{1,0:T(8,128)(2,1)} async-done(((bf16[128,2816]{1,0:T(8,128)(2,1)}), bf16[2048,2816]{1,0:T(8,128)(2,1)}) %all-gather.10.cloned.1.call-update) | async-done | bytes 11534352 | tf_op jit(solution)/shard_map/all_gather | solution.py:39
  296.7 183.0 %all-gather.12.cloned.1.call-done = bf16[2816,2048]{1,0:T(8,128)(2,1)} async-done(((bf16[2816,128]{1,0:T(8,128)(2,1)}), bf16[2816,2048]{1,0:T(8,128)(2,1)}) %all-gather.12.cloned.1.call-update) | async-done | bytes 11534352 | tf_op jit(solution)/shard_map/all_gather | solution.py:33
  479.6 17.5 %convolution_convert_fusion.2 = bf16[320,2048]{1,0:T(8,128)(2,1)} fusion(bf16[2816,2048]{1,0:T(8,128)(2,1)} %all-gather.12.cloned.1.call-done, bf16[2048,2816]{1,0:T(8,128)(2,1)} %all-gather.10.cloned.1.call-done, f32[320,2816]{1,0:T(8,128)} %fusion.23, f32[2048]{0:T(1024)S(1)} %bitcast.41, f32[320]{0:T(512)S(1)} %add_rsqrt_fusion, ...), kind=kOutput, calls=%fused_computation.6 | convolution fusion | flops 7390658560 | bytes 29304064 | tf_op jit(solution)/shard_map/dot_general | solution.py:15
  497.1 0.0 reduce-scatter.4.cloned.1.call-update
  497.1 0.0 all-gather.16.cloned.1.call-start
  497.2 0.5 all-gather.16.cloned.1.call-update
  497.7 0.0 all-gather.14.cloned.1.call-start
  497.8 1.9 convert_element_type.82
  499.6 4.5 reduce-scatter.4.cloned.1.call-done
  504.1 1.3 fusion.2
  505.4 2.0 multiply_reduce_fusion.2
  507.4 1.0 multiply_convert_fusion.2
  508.5 0.0 all-gather.14.cloned.1.call-update
  508.5 0.0 all-gather.18.cloned.1.call-start
  508.5 0.7 all-gather.18.cloned.1.call-update
  509.2 0.0 reduce-scatter.6.cloned.1.call-start
  509.4 59.1 %all-gather.16.cloned.1.call-done = bf16[2048,512]{1,0:T(8,128)(2,1)} async-done(((bf16[128,512]{1,0:T(8,128)(2,1)}), bf16[2048,512]{1,0:T(8,128)(2,1)}) %all-gather.16.cloned.1.call-update) | async-done | bytes 2097168 | tf_op jit(solution)/shard_map/all_gather | solution.py:34
  568.5 9.6 %all-gather.14.cloned.1.call-done = bf16[320,2048]{1,0:T(8,128)(2,1)} async-done(((bf16[160,2048]{1,0:T(8,128)(2,1)}), bf16[320,2048]{1,0:T(8,128)(2,1)}) %all-gather.14.cloned.1.call-update) | async-done | bytes 1310736 | tf_op jit(solution)/shard_map/all_gather | solution.py:23
  578.1 2.8 fusion.14
  580.9 0.2 reshape.106
  581.2 0.1 fusion.33
  581.3 1.6 fusion.22
  582.9 0.2 convolution_bitcast_fusion
  583.2 0.4 copy.12
  583.6 61.4 %all-gather.18.cloned.1.call-done = bf16[512,2048]{1,0:T(8,128)(2,1)} async-done(((bf16[512,128]{1,0:T(8,128)(2,1)}), bf16[512,2048]{1,0:T(8,128)(2,1)}) %all-gather.18.cloned.1.call-update) | async-done | bytes 2097168 | tf_op jit(solution)/shard_map/all_gather | solution.py:35
  645.0 3.6 convolution_convert_fusion
  648.5 0.0 reduce-scatter.6.cloned.1.call-update
  648.5 0.2 all-gather.20.cloned.1.call-start
  648.8 6.8 reduce-scatter.6.cloned.1.call-done
  655.6 1.4 fusion.6
  656.9 1.5 multiply_reduce_fusion.1
  658.4 1.2 multiply_convert_fusion.1
  659.7 0.0 reduce-scatter.8.cloned.1.call-start
  659.7 10.8 %all-gather.20.cloned.1.call-done = bf16[320,2048]{1,0:T(8,128)(2,1)} async-done(((bf16[160,2048]{1,0:T(8,128)(2,1)}), bf16[320,2048]{1,0:T(8,128)(2,1)}) %all-gather.20.cloned.1.call-update) | async-done | bytes 1310736 | tf_op jit(solution)/shard_map/all_gather | solution.py:23
  670.6 10.4 %fusion.34 = f32[320,2816]{1,0:T(8,128)} fusion(bf16[320,2048]{1,0:T(8,128)(2,1)} %all-gather.20.cloned.1.call-done, bf16[2048,2816]{1,0:T(8,128)(2,1)} %all-gather.8.cloned.1.call-done), kind=kOutput, calls=%fused_computation.77 | convolution fusion | flops 3690987520 | bytes 16449536 | tf_op jit(solution)/shard_map/dot_general | solution.py:75
  681.0 17.7 %convolution_convert_fusion.1 = bf16[320,2048]{1,0:T(8,128)(2,1)} fusion(bf16[2816,2048]{1,0:T(8,128)(2,1)} %all-gather.12.cloned.1.call-done, bf16[320,2048]{1,0:T(8,128)(2,1)} %all-gather.20.cloned.1.call-done, bf16[2048,2816]{1,0:T(8,128)(2,1)} %all-gather.10.cloned.1.call-done, f32[320,2816]{1,0:T(8,128)} %fusion.34), kind=kOutput, calls=%fused_computation.5 | convolution fusion | flops 7388037120 | bytes 29294592 | tf_op jit(solution)/shard_map/dot_general | solution.py:15
  698.7 10.0 %reduce-scatter.8.cloned.1.call-done = bf16[160,2048]{1,0:T(8,128)(2,1)} async-done(((bf16[320,2048]{1,0:T(8,128)(2,1)}), bf16[160,2048]{1,0:T(8,128)(2,1)}) %reduce-scatter.8.cloned.1.call-update) | async-done | bytes 655376 | tf_op jit(solution)/shard_map/reduce_scatter | solution.py:14
  708.8 1.3 fusion.9
  710.1 2.4 fusion.13
  (27 shorter events, 0.2 us)
Async XLA Ops:
  6.5 576.4 %copy-start = (bf16[4,128,128]{2,1,0:T(8,128)(2,1)S(1)}, bf16[4,128,128]{2,1,0:T(8,128)(2,1)}, u32[]{:S(2)}) copy-start(bf16[4,128,128]{2,1,0:T(8,128)(2,1)} %param.15) | copy-start | bytes 393220
  6.5 2.3 copy-start.3
  6.5 147.7 %all-gather.8.cloned.1.call-start = ((), (), s32[]{:S(2)}) async-start(), calls=%async_computation.3 | async-start | bytes 12255232 | tf_op jit(solution)/shard_map/all_gather | solution.py:38
  7.3 1.9 copy-start.4
  7.3 289.4 %all-gather.10.cloned.1.call-start = ((), (), s32[]{:S(2)}) async-start(), calls=%async_computation.4 | async-start | bytes 12255232 | tf_op jit(solution)/shard_map/all_gather | solution.py:39
  8.0 471.6 %all-gather.12.cloned.1.call-start = ((), (), s32[]{:S(2)}) async-start(), calls=%async_computation.5 | async-start | bytes 12255232 | tf_op jit(solution)/shard_map/all_gather | solution.py:33
  8.8 495.4 %reduce-scatter.4.cloned.1.call-start = ((), (), s32[]{:S(2)}) async-start(), calls=%async_computation.6 | async-start | bytes 1966080 | tf_op jit(solution)/shard_map/reduce_scatter | solution.py:14
  497.1 71.3 %all-gather.16.cloned.1.call-start = ((), (), s32[]{:S(2)}) async-start(), calls=%async_computation.8 | async-start | bytes 2228224 | tf_op jit(solution)/shard_map/all_gather | solution.py:34
  497.7 80.4 %all-gather.14.cloned.1.call-start = ((), (), s32[]{:S(2)}) async-start(), calls=%async_computation.7 | async-start | bytes 1966080 | tf_op jit(solution)/shard_map/all_gather | solution.py:23
  507.4 1.9 copy-start.5
  508.5 136.5 %all-gather.18.cloned.1.call-start = ((), (), s32[]{:S(2)}) async-start(), calls=%async_computation.9 | async-start | bytes 2228224 | tf_op jit(solution)/shard_map/all_gather | solution.py:35
  509.2 146.3 %reduce-scatter.6.cloned.1.call-start = ((), (), s32[]{:S(2)}) async-start(), calls=%async_computation.10 | async-start | bytes 1966080 | tf_op jit(solution)/shard_map/reduce_scatter | solution.py:14
  648.5 22.0 %all-gather.20.cloned.1.call-start = ((), (), s32[]{:S(2)}) async-start(), calls=%async_computation.11 | async-start | bytes 1966080 | tf_op jit(solution)/shard_map/all_gather | solution.py:23
  655.6 2.9 copy-start.2
  659.7 49.1 %reduce-scatter.8.cloned.1.call-start = ((), (), s32[]{:S(2)}) async-start(), calls=%async_computation.12 | async-start | bytes 1966080 | tf_op jit(solution)/shard_map/reduce_scatter | solution.py:14
  710.1 2.4 copy-start.1
Sparse Core Ops, SparseCore 0:
  10.1 144.1 all-gather.7
  157.0 139.5 all-gather.9
  299.4 180.2 all-gather.11
  497.2 6.8 reduce-scatter.3
  506.8 61.6 all-gather.15
  569.9 8.1 all-gather.13
  580.8 64.0 all-gather.17
  648.7 6.8 reduce-scatter.5
  659.8 10.7 all-gather.19
  698.9 9.8 reduce-scatter.7
where the time goes:
time: 720 us; the launch traced here: 719 us
  waiting for transfers between devices  627 us (87%)
  matrix products  60.9 us (8%)
  other arithmetic  16.1 us (2%)
  between operations  13.7 us (2%)
    all_gather x1, waiting for transfers between devices, body(): lax.all_gather(w_down, 'fs', axis=1, tiled=True)  183 us
    all_gather x1, waiting for transfers between devices, body(): lax.all_gather(w_gate, 'fs', axis=0, tiled=True)  145 us
    all_gather x1, waiting for transfers between devices, body(): lax.all_gather(w_up, 'fs', axis=0, tiled=True)  134 us
    all_gather x1, waiting for transfers between devices, body(): lax.all_gather(w_mix_out, 'fs', axis=1, tiled=True)  61.4 us
    all_gather x1, waiting for transfers between devices, body(): lax.all_gather(w_mix_in, 'fs', axis=0, tiled=True)  59.1 us
    dot_general x3, matrix products, reduce_rows(): jnp.dot(left_rows, right_matrix, preferred_element_type=jnp.float32)  38.7 us
    reduce_scatter x3, waiting for transfers between devices, reduce_rows(): lax.psum_scatter(jnp.dot(left_rows, right_matrix, preferred_element_type=...  21.3 us
    all_gather x2, waiting for transfers between devices, gather_rows(): lax.all_gather(normed, 'tp', axis=0, tiled=True)  20.5 us
  transfers between devices with their start and end apart: 10, of which 10 were waited for; matrix products, arithmetic and copies ran while one was open for 3% of the time, Pallas kernels for 0%

commit v1 on v0

--- a/solution.py
+++ b/solution.py
@@ -1,9 +1,310 @@
+import functools
+import itertools
+
 import jax
 import jax.numpy as jnp
 from jax import lax
+from jax.experimental import pallas as pl
+from jax.experimental.pallas import tpu as pltpu
 from jax.sharding import PartitionSpec as P
 
 LEN = 64
+MESH = pl.DeviceIdType.MESH
+
+
+def line_dims(mesh):
+    devices = mesh.devices.reshape(mesh.shape["fs"], -1)[:, 0]
+    count = len(devices)
+    coords = [tuple(getattr(d, "coords", ())) for d in devices]
+    dims = []
+    for axis in range(len(coords[0])):
+        values = sorted({c[axis] for c in coords})
+        if len(values) > 1:
+            stride = next(i for i in range(count) if coords[i][axis] != coords[0][axis])
+            dims.append((len(values), stride, axis, values))
+    dims.sort(key=lambda d: -d[1])
+    good = len(dims) > 0 and all(
+        sum(vals.index(c[axis]) * stride for _, stride, axis, vals in dims) == i
+        for i, c in enumerate(coords)
+    )
+    if not good:
+        return ((count, 1),)
+    return tuple((d[0], d[1]) for d in dims)
+
+
+def near(position, size, rank):
+    inner = jnp.minimum(position, size - 1 - position)
+    alternating = rank <= 2 * inner
+    distance = jnp.where(alternating, (rank + 1) // 2, rank - inner)
+    toward_high = jnp.where(alternating, rank % 2 == 1, 2 * position < size - 1)
+    step = jnp.where(toward_high, 1, -1)
+    return position + step * distance, -step
+
+
+def piece_plan(dims, order):
+    sizes = [dims[d][0] for d in order]
+    slots = []
+    for ranks in itertools.product(*[range(n) for n in sizes]):
+        slots.append(ranks)
+    slots.sort(key=lambda r: (sum(r), r))
+    return slots
+
+
+class Piece:
+    def __init__(self, index, dims, order, src_of, dst_of):
+        self.index, self.dims, self.order = index, dims, order
+        self.src_of, self.dst_of = src_of, dst_of
+        self.slots = piece_plan(dims, order)
+
+    def locate(self, me, ranks):
+        source, last, away = me, -1, None
+        for place, (d, rank) in enumerate(zip(self.order, ranks)):
+            if rank > 0:
+                size, stride = self.dims[d]
+                position = (me // stride) % size
+                found, step = near(position, size, rank)
+                source = source + (found - position) * stride
+                last, away = place, step
+        return source, last, away
+
+    def sends(self, me, ranks):
+        _, last, away = self.locate(me, ranks)
+        out = []
+        for place, d in enumerate(self.order):
+            size, stride = self.dims[d]
+            position = (me // stride) % size
+            if place == last:
+                if size > 2:
+                    ok = jnp.logical_and(position + away >= 0, position + away < size)
+                    out.append((ok, me + away * stride))
+            elif place > last:
+                if size == 2:
+                    out.append((None, me + (1 - 2 * position) * stride))
+                else:
+                    out.append((position + 1 < size, me + stride))
+                    out.append((position > 0, me - stride))
+        return out
+
+
+def when(condition, act):
+    if condition is None:
+        act()
+    else:
+        pl.when(condition)(act)
+
+
+def spread(pieces, me, chunk, send_sem, recv_sem, low, high, mode):
+    todo = []
+    for piece in pieces:
+        for ranks in piece.slots:
+            todo.append((sum(ranks), piece, ranks))
+    todo.sort(key=lambda t: t[0])
+    for depth, piece, ranks in todo:
+        if not low <= depth < high:
+            continue
+        source, last, _ = piece.locate(me, ranks)
+        landed = piece.dst_of(chunk, source)
+        origin = piece.src_of(chunk) if depth == 0 else landed
+        recv = recv_sem.at[chunk, piece.index, source]
+        if depth > 0 and mode == "start":
+            pltpu.make_async_copy(landed, landed, recv).wait()
+        base = piece.first_send[ranks]
+        for offset, (ok, target) in enumerate(piece.sends(me, ranks)):
+            copy = pltpu.make_async_remote_copy(
+                src_ref=origin,
+                dst_ref=landed,
+                send_sem=send_sem.at[chunk, base + offset],
+                recv_sem=recv,
+                device_id={"fs": target},
+                device_id_type=MESH,
+            )
+            when(ok, copy.start if mode == "start" else copy.wait_send)
+
+
+def number_sends(pieces):
+    total = 0
+    for piece in pieces:
+        piece.first_send = {}
+        for ranks in piece.slots:
+            piece.first_send[ranks] = total
+            last = max([i for i, r in enumerate(ranks) if r > 0], default=-1)
+            for place, d in enumerate(piece.order):
+                size = piece.dims[d][0]
+                if place == last:
+                    total += 1 if size > 2 else 0
+                elif place > last:
+                    total += 1 if size == 2 else 2
+    return total
+
+
+def cut(extent, unit, share):
+    return max(unit, min(extent - unit, round(extent * share / unit) * unit))
+
+
+def gather_plan(dims, refs, outs, block, blocks):
+    gate, up, down, mix_in, mix_out = refs
+    gate_o, up_o, down_o, mix_in_o, mix_out_o = outs
+    n = len(dims)
+    first = tuple(range(n))
+    second = first[1:] + first[:1]
+    third = first[-1:] + first[:-1]
+    depth, width = gate.shape
+    across = down.shape[1]
+    mixed = mix_in.shape[1]
+    pooled = mix_out.shape[0]
+
+    def columns(ref, out, start_of, size):
+        return (
+            lambda c: ref.at[:, pl.ds(start_of(c), size)],
+            lambda c, s: out.at[pl.ds(s * depth, depth), pl.ds(start_of(c), size)],
+        )
+
+    def rows(ref, out, start_of, size):
+        def dst(c, s):
+            if len(out.shape) == 3:
+                return out.at[s, pl.ds(start_of(c), size), :]
+            return out.at[pl.ds(start_of(c), size), pl.ds(s * across, across)]
+
+        return (lambda c: ref.at[pl.ds(start_of(c), size), :], dst)
+
+    def at(offset):
+        if blocks == 1:
+            return lambda c: offset
+        return lambda c: pl.multiple_of(c * block + offset, 16 if offset else block)
+
+    down_cut = cut(block, 16, 2 / 3)
+    main = [
+        Piece(0, dims, first, *columns(gate, gate_o, at(0), block)),
+        Piece(1, dims, third, *columns(up, up_o, at(0), block)),
+        Piece(2, dims, first, *rows(down, down_o, at(0), down_cut)),
+        Piece(3, dims, second, *rows(down, down_o, at(down_cut), block - down_cut)),
+    ]
+    mix_cut = cut(pooled, 16, 2 / 3)
+
+    def fixed(offset):
+        return lambda c: offset
+
+    mix = [
+        Piece(0, dims, first, *columns(mix_in, mix_in_o, fixed(0), mixed)),
+        Piece(1, dims, third, *rows(mix_out, mix_out_o, fixed(0), mix_cut)),
+        Piece(2, dims, second, *rows(mix_out, mix_out_o, fixed(mix_cut), pooled - mix_cut)),
+    ]
+    return main, mix
+
+
+def gather_kernel(dims, block, blocks, *args):
+    refs, outs = args[:5], args[5:10]
+    send_sem, recv_sem, local_sem = args[10:]
+    me = lax.axis_index("fs")
+    barrier = pltpu.get_barrier_semaphore()
+    expected = 0
+    for size, stride in dims:
+        position = (me // stride) % size
+        for step, ok in ((1, position + 1 < size), (-1, position > 0)):
+            def signal(step=step, stride=stride):
+                pl.semaphore_signal(
+                    barrier, inc=1, device_id={"fs": me + step * stride}, device_id_type=MESH
+                )
+
+            pl.when(ok)(signal)
+            expected = expected + jnp.where(ok, 1, 0)
+    pl.semaphore_wait(barrier, expected)
+
+    main, mix = gather_plan(dims, refs, outs, block, blocks)
+    number_sends(main)
+    number_sends(mix)
+    deepest = sum(size - 1 for size, _ in dims) + 1
+    early = min(3, deepest)
+
+    locals_ = []
+    for i, (ref, out) in enumerate(zip(refs, outs)):
+        rows_here, columns_here = ref.shape
+        if len(out.shape) == 3:
+            target = out.at[me]
+        elif i in (0, 1, 3):
+            target = out.at[pl.ds(me * rows_here, rows_here), :]
+        else:
+            target = out.at[:, pl.ds(me * columns_here, columns_here)]
+        locals_.append(pltpu.make_async_copy(ref, target, local_sem.at[i]))
+
+    go = functools.partial(spread, send_sem=send_sem, recv_sem=recv_sem)
+    go(main, me, 0, low=0, high=1, mode="start")
+    for copy in locals_:
+        copy.start()
+
+    def step(i, carry):
+        @pl.when(i + 1 < blocks)
+        def _():
+            go(main, me, i + 1, low=0, high=1, mode="start")
+
+        go(main, me, i, low=1, high=early, mode="start")
+
+        @pl.when(i > 0)
+        def _():
+            go(main, me, i - 1, low=early, high=deepest, mode="start")
+
+        return carry
+
+    lax.fori_loop(0, blocks, step, 0)
+    go(mix, me, blocks, low=0, high=1, mode="start")
+    go(main, me, blocks - 1, low=early, high=deepest, mode="start")
+    go(mix, me, blocks, low=1, high=deepest, mode="start")
+
+    def finish(i, carry):
+        go(main, me, i, low=0, high=deepest, mode="end")
+        return carry
+
+    lax.fori_loop(0, blocks, finish, 0)
+    go(mix, me, blocks, low=0, high=deepest, mode="end")
+    for copy in locals_:
+        copy.wait()
+
+
+def gather_weights(dims, w_gate, w_up, w_down, w_mix_in, w_mix_out):
+    count = 1
+    for size, _ in dims:
+        count *= size
+    width = w_gate.shape[1]
+    block = next((b for b in (256, 128) if width % b == 0), width)
+    blocks = width // block
+
+    def rows_out(a):
+        return jax.ShapeDtypeStruct((a.shape[0] * count, a.shape[1]), a.dtype)
+
+    def columns_out(a):
+        if a.shape[1] % 128 == 0:
+            return jax.ShapeDtypeStruct((a.shape[0], a.shape[1] * count), a.dtype)
+        return jax.ShapeDtypeStruct((count, *a.shape), a.dtype)
+
+    shapes = [rows_out(w_gate), rows_out(w_up), columns_out(w_down)]
+    shapes += [rows_out(w_mix_in), columns_out(w_mix_out)]
+    class Shape:
+        def __init__(self, shape):
+            self.shape = shape
+
+    stand_in = [Shape(a.shape) for a in (w_gate, w_up, w_down, w_mix_in, w_mix_out)]
+    main, mix = gather_plan(dims, stand_in, [Shape(s.shape) for s in shapes], block, blocks)
+    sends = max(number_sends(main), number_sends(mix))
+    outs = pl.pallas_call(
+        functools.partial(gather_kernel, dims, block, blocks),
+        out_shape=shapes,
+        in_specs=[pl.BlockSpec(memory_space=pltpu.HBM)] * 5,
+        out_specs=[pl.BlockSpec(memory_space=pltpu.HBM)] * 5,
+        scratch_shapes=[
+            pltpu.SemaphoreType.DMA((blocks + 1, sends)),
+            pltpu.SemaphoreType.DMA((blocks + 1, len(main), count)),
+            pltpu.SemaphoreType.DMA((5,)),
+        ],
+        compiler_params=pltpu.CompilerParams(collective_id=0, has_side_effects=True),
+        name="gather_weights",
+    )(w_gate, w_up, w_down, w_mix_in, w_mix_out)
+
+    def flat(a):
+        if a.ndim == 2:
+            return a
+        return jnp.transpose(a, (1, 0, 2)).reshape(a.shape[1], -1)
+
+    return [flat(a) for a in outs]
 
 
 def rms_scale(values, gain):
@@ -23,20 +324,14 @@
     return project(lax.all_gather(normed, "tp", axis=0, tiled=True), jnp.int32(0))
 
 
-def body(tokens, w_gate, w_up, w_down, w_mix_in, w_mix_out, pool_w, pool_scale, norm_gains):
+def body(dims, tokens, w_gate, w_up, w_down, w_mix_in, w_mix_out, pool_w, pool_scale, norm_gains):
     tp_size = lax.axis_size("tp")
     rows_all = tokens.shape[0]
     own_rows = rows_all // tp_size
     stream = tokens.astype(jnp.float32)
     normed = rms_scale(stream, norm_gains[0]).astype(jnp.bfloat16)
-    down_full, mix_in_full, mix_out_full = (
-        lax.all_gather(w_down, "fs", axis=1, tiled=True),
-        lax.all_gather(w_mix_in, "fs", axis=0, tiled=True),
-        lax.all_gather(w_mix_out, "fs", axis=1, tiled=True),
-    )
-    gate_full, up_full = (
-        lax.all_gather(w_gate, "fs", axis=0, tiled=True),
-        lax.all_gather(w_up, "fs", axis=0, tiled=True),
+    gate_full, up_full, down_full, mix_in_full, mix_out_full = gather_weights(
+        dims, w_gate, w_up, w_down, w_mix_in, w_mix_out
     )
     gate_first = jnp.dot(normed, gate_full, preferred_element_type=jnp.float32)
     up_first = jnp.dot(normed, up_full, preferred_element_type=jnp.float32)
@@ -94,4 +389,4 @@
         P(),
     )
     out_specs = P(("fs", "tp"), None)
-    return jax.shard_map(body, mesh=mesh, in_specs=in_specs, out_specs=out_specs, check_vma=False)
+    return jax.shard_map(functools.partial(body, line_dims(mesh)), mesh=mesh, in_specs=in_specs, out_specs=out_specs, check_vma=False)

time: 720 us -> 462 us (0.64)
  waiting for transfers between devices: 627 us -> 48.8 us
  Pallas kernels: 0 us -> 319 us
    all_gather x5 -> x0, waiting for transfers between devices: 582 us -> none  [the longest x1 183 us: body(): lax.all_gather(w_down, 'fs', axis=1, tiled=True)]
    pallas_call x0 -> x1, Pallas kernels: none -> 319 us  [gather_weights(): pl.pallas_call(functools.partial(gather_kernel, dims, block, blocks), out...]
  transfers between devices with their start and end apart: 10 -> 5, of which waited for: 10 -> 5; matrix products, arithmetic and copies ran while one was open for 3% -> 0% of each run, Pallas kernels for 0% -> 0%
where the time goes in v1:
time: 462 us; the launch traced here: 461 us
  Pallas kernels  319 us (69%)
  matrix products  59.4 us (13%)
  waiting for transfers between devices  48.8 us (11%)
  other arithmetic  17.4 us (4%)
  between operations  13.3 us (3%)
    pallas_call x1, Pallas kernels, gather_weights(): pl.pallas_call(functools.partial(gather_kernel, dims, block, blocks), out...  319 us
    dot_general x3, matrix products, reduce_rows(): jnp.dot(left_rows, right_matrix, preferred_element_type=jnp.float32)  37.1 us
    reduce_scatter x3, waiting for transfers between devices, reduce_rows(): lax.psum_scatter(jnp.dot(left_rows, right_matrix, preferred_element_type=...  27.2 us
    all_gather x2, waiting for transfers between devices, gather_rows(): lax.all_gather(normed, 'tp', axis=0, tiled=True)  21.5 us
    dot_general x1, matrix products, project_ffn(): jnp.dot(part_rows, gate_full, preferred_element_type=jnp.float32)  10.5 us
  transfers between devices with their start and end apart: 5, of which 5 were waited for; matrix products, arithmetic and copies ran while one was open for 0% of the time, Pallas kernels for 0%

profile of v1, /device:TPU:0, one launch (start us, length us, event | category | flops | bytes accessed | tf_op | source)
XLA Modules:
  0.0 461.2 jit_solution(18065971164695198082)
XLA Ops:
  6.5 0.0 copy-start
  6.5 0.0 reduce-scatter.4.cloned.1.call-start
  6.5 1.1 fusion.32
  7.7 1.7 multiply_reduce_fusion
  9.3 0.0 copy-start.3
  9.4 319.3 %gather_weights.1 = (bf16[2048,2816]{1,0:T(8,128)(2,1)}, bf16[2048,2816]{1,0:T(8,128)(2,1)}, bf16[2816,2048]{1,0:T(8,128)(2,1)}, bf16[2048,512]{1,0:T(8,128)(2,1)}, bf16[512,2048]{1,0:T(8,128)(2,1)}) custom-call(bf16[128,2816]{1,0:T(8,128)(2,1)} %args_0_.4, bf16[128,2816]{1,0:T(8,128)(2,1)} %args_1_.4, bf16[2816,128]{1,0:T(8,128)(2,1)} %args_2_.4, ...), custom_call_target="tpu_custom_call" | custom-call | tf_op jit(solution)/shard_map/gather_weights/pallas_call | solution.py:288
  328.7 0.0 copy-done.3
  328.7 8.7 %fusion.23 = f32[320,2816]{1,0:T(8,128)} fusion(bf16[2048,2816]{1,0:T(8,128)(2,1)} %get-tuple-element.10, f32[2048]{0:T(1024)S(1)} %bitcast.40, f32[320]{0:T(512)S(1)} %add_rsqrt_fusion, bf16[320,2048]{1,0:T(8,128)(2,1)S(1)} %copy-done.3), kind=kOutput, calls=%fused_computation.50 | convolution fusion | flops 3693608960 | bytes 16459008 | tf_op jit(solution)/shard_map/dot_general | solution.py:336
  337.4 17.4 %convolution_convert_fusion.2 = bf16[320,2048]{1,0:T(8,128)(2,1)} fusion(bf16[2816,2048]{1,0:T(8,128)(2,1)} %get-tuple-element.12, bf16[2048,2816]{1,0:T(8,128)(2,1)} %get-tuple-element.11, f32[320,2816]{1,0:T(8,128)} %fusion.23, f32[2048]{0:T(1024)S(1)} %bitcast.41, f32[320]{0:T(512)S(1)} %add_rsqrt_fusion, bf16[320,2048]{1,0:T(8,128)(2,1)S(1)} %copy-done.3), kind=kOutput, calls=%fused_computation.6 | convolution fusion | flops 7390658560 | bytes 29304064 | tf_op jit(solution)/shard_map/dot_general | solution.py:316
  354.9 0.0 reduce-scatter.4.cloned.1.call-update
  354.9 0.2 all-gather.3.cloned.1.call-start
  355.1 1.8 convert_element_type.82
  356.9 7.2 %reduce-scatter.4.cloned.1.call-done = bf16[160,2048]{1,0:T(8,128)(2,1)} async-done(((bf16[320,2048]{1,0:T(8,128)(2,1)}), bf16[160,2048]{1,0:T(8,128)(2,1)}) %reduce-scatter.4.cloned.1.call-update) | async-done | bytes 655376 | tf_op jit(solution)/shard_map/reduce_scatter | solution.py:315
  364.1 1.3 fusion.2
  365.4 2.0 multiply_reduce_fusion.2
  367.4 0.0 copy-start.4
  367.4 1.0 multiply_convert_fusion.2
  368.4 0.0 all-gather.3.cloned.1.call-update
  368.5 0.0 reduce-scatter.6.cloned.1.call-start
  368.5 0.0 copy-done.4
  368.6 10.7 %all-gather.3.cloned.1.call-done = bf16[320,2048]{1,0:T(8,128)(2,1)} async-done(((bf16[160,2048]{1,0:T(8,128)(2,1)}), bf16[320,2048]{1,0:T(8,128)(2,1)}) %all-gather.3.cloned.1.call-update) | async-done | bytes 1310736 | tf_op jit(solution)/shard_map/all_gather | solution.py:324
  379.3 2.8 fusion.14
  382.2 0.2 reshape.106
  382.4 0.1 fusion.33
  382.5 1.6 fusion.22
  384.1 0.0 copy-done
  384.1 0.0 copy-start.5
  384.1 0.2 convolution_bitcast_fusion
  384.4 0.4 copy.12
  384.8 0.9 copy-done.5
  385.7 1.9 convolution_convert_fusion
  387.7 0.0 reduce-scatter.6.cloned.1.call-update
  387.7 0.0 all-gather.5.cloned.1.call-start
  387.7 10.0 %reduce-scatter.6.cloned.1.call-done = bf16[160,2048]{1,0:T(8,128)(2,1)} async-done(((bf16[320,2048]{1,0:T(8,128)(2,1)}), bf16[160,2048]{1,0:T(8,128)(2,1)}) %reduce-scatter.6.cloned.1.call-update) | async-done | bytes 655376 | tf_op jit(solution)/shard_map/reduce_scatter | solution.py:315
  397.7 1.4 fusion.6
  399.1 1.5 multiply_reduce_fusion.1
  400.6 0.0 copy-done.2
  400.6 1.2 multiply_convert_fusion.1
  401.8 0.0 all-gather.5.cloned.1.call-update
  401.8 0.0 reduce-scatter.8.cloned.1.call-start
  401.9 10.8 %all-gather.5.cloned.1.call-done = bf16[320,2048]{1,0:T(8,128)(2,1)} async-done(((bf16[160,2048]{1,0:T(8,128)(2,1)}), bf16[320,2048]{1,0:T(8,128)(2,1)}) %all-gather.5.cloned.1.call-update) | async-done | bytes 1310736 | tf_op jit(solution)/shard_map/all_gather | solution.py:324
  412.7 10.5 %fusion.34 = f32[320,2816]{1,0:T(8,128)} fusion(bf16[320,2048]{1,0:T(8,128)(2,1)} %all-gather.5.cloned.1.call-done, bf16[2048,2816]{1,0:T(8,128)(2,1)} %get-tuple-element.10), kind=kOutput, calls=%fused_computation.77 | convolution fusion | flops 3690987520 | bytes 16449536 | tf_op jit(solution)/shard_map/dot_general | solution.py:370
  423.2 17.7 %convolution_convert_fusion.1 = bf16[320,2048]{1,0:T(8,128)(2,1)} fusion(bf16[2816,2048]{1,0:T(8,128)(2,1)} %get-tuple-element.12, bf16[320,2048]{1,0:T(8,128)(2,1)} %all-gather.5.cloned.1.call-done, bf16[2048,2816]{1,0:T(8,128)(2,1)} %get-tuple-element.11, f32[320,2816]{1,0:T(8,128)} %fusion.34), kind=kOutput, calls=%fused_computation.5 | convolution fusion | flops 7388037120 | bytes 29294592 | tf_op jit(solution)/shard_map/dot_general | solution.py:316
  440.9 0.0 reduce-scatter.8.cloned.1.call-update
  440.9 10.0 %reduce-scatter.8.cloned.1.call-done = bf16[160,2048]{1,0:T(8,128)(2,1)} async-done(((bf16[320,2048]{1,0:T(8,128)(2,1)}), bf16[160,2048]{1,0:T(8,128)(2,1)}) %reduce-scatter.8.cloned.1.call-update) | async-done | bytes 655376 | tf_op jit(solution)/shard_map/reduce_scatter | solution.py:315
  450.9 1.3 fusion.9
  452.2 2.4 fusion.13
  454.7 0.0 copy-done.1
  (13 shorter events, 0.1 us)
Async XLA Ops:
  6.5 377.6 %copy-start = (bf16[4,128,128]{2,1,0:T(8,128)(2,1)S(1)}, bf16[4,128,128]{2,1,0:T(8,128)(2,1)}, u32[]{:S(2)}) copy-start(bf16[4,128,128]{2,1,0:T(8,128)(2,1)} %param.15) | copy-start | bytes 393220
  6.5 357.6 %reduce-scatter.4.cloned.1.call-start = ((), (), s32[]{:S(2)}) async-start(), calls=%async_computation.3 | async-start | bytes 1966080 | tf_op jit(solution)/shard_map/reduce_scatter | solution.py:315
  9.3 319.3 %copy-start.3 = (bf16[320,2048]{1,0:T(8,128)(2,1)S(1)}, bf16[320,2048]{1,0:T(8,128)(2,1)}, u32[]{:S(2)}) copy-start(bf16[320,2048]{1,0:T(8,128)(2,1)} %param.9) | copy-start | bytes 3932164
  354.9 24.4 %all-gather.3.cloned.1.call-start = ((), (), s32[]{:S(2)}) async-start(), calls=%async_computation.4 | async-start | bytes 1966080 | tf_op jit(solution)/shard_map/all_gather | solution.py:324
  367.4 1.1 copy-start.4
  368.5 29.2 %reduce-scatter.6.cloned.1.call-start = ((), (), s32[]{:S(2)}) async-start(), calls=%async_computation.5 | async-start | bytes 1966080 | tf_op jit(solution)/shard_map/reduce_scatter | solution.py:315
  384.1 1.6 copy-start.5
  387.7 25.0 %all-gather.5.cloned.1.call-start = ((), (), s32[]{:S(2)}) async-start(), calls=%async_computation.6 | async-start | bytes 1966080 | tf_op jit(solution)/shard_map/all_gather | solution.py:324
  397.7 2.9 copy-start.2
  401.8 49.1 %reduce-scatter.8.cloned.1.call-start = ((), (), s32[]{:S(2)}) async-start(), calls=%async_computation.7 | async-start | bytes 1966080 | tf_op jit(solution)/shard_map/reduce_scatter | solution.py:315
  452.2 2.4 copy-start.1
Sparse Core Ops, SparseCore 0:
  355.0 9.0 reduce-scatter.3
  368.6 10.6 all-gather.2
  387.8 9.8 reduce-scatter.5
  402.0 10.6 all-gather.4
  441.0 9.8 reduce-scatter.7

commit v2 on v1

--- a/solution.py
+++ b/solution.py
@@ -311,23 +311,34 @@
     return values * lax.rsqrt(jnp.mean(values * values, axis=-1, keepdims=True) + 1e-06) * gain
 
 
-def reduce_rows(left_rows, right_matrix):
-    return lax.psum_scatter(
-        jnp.dot(left_rows, right_matrix, preferred_element_type=jnp.float32).astype(jnp.bfloat16),
-        "tp",
-        scatter_dimension=0,
-        tiled=True,
-    ).astype(jnp.float32)
-
-
-def gather_rows(normed, project):
-    return project(lax.all_gather(normed, "tp", axis=0, tiled=True), jnp.int32(0))
+def total_over_tp(left_rows, right_matrix):
+    part = jnp.dot(left_rows, right_matrix, preferred_element_type=jnp.float32)
+    part = part.astype(jnp.bfloat16)
+    if lax.axis_size("tp") == 2:
+        other = lax.ppermute(part, "tp", ((0, 1), (1, 0)))
+        return part.astype(jnp.float32) + other.astype(jnp.float32)
+    return lax.psum(part.astype(jnp.float32), "tp")
+
+
+def own_total_over_tp(left_rows, right_matrix):
+    part = jnp.dot(left_rows, right_matrix, preferred_element_type=jnp.float32)
+    part = part.astype(jnp.bfloat16)
+    if lax.axis_size("tp") == 2:
+        mine = own_rows_of(part)
+        half = mine.shape[0]
+        theirs = lax.dynamic_slice_in_dim(part, (1 - lax.axis_index("tp")) * half, half, 0)
+        other = lax.ppermute(theirs, "tp", ((0, 1), (1, 0)))
+        return mine.astype(jnp.float32) + other.astype(jnp.float32)
+    return lax.psum_scatter(part.astype(jnp.float32), "tp", scatter_dimension=0, tiled=True)
+
+
+def own_rows_of(array):
+    count = array.shape[0] // lax.axis_size("tp")
+    return lax.dynamic_slice_in_dim(array, lax.axis_index("tp") * count, count, 0)
 
 
 def body(dims, tokens, w_gate, w_up, w_down, w_mix_in, w_mix_out, pool_w, pool_scale, norm_gains):
-    tp_size = lax.axis_size("tp")
     rows_all = tokens.shape[0]
-    own_rows = rows_all // tp_size
     stream = tokens.astype(jnp.float32)
     normed = rms_scale(stream, norm_gains[0]).astype(jnp.bfloat16)
     gate_full, up_full, down_full, mix_in_full, mix_out_full = gather_weights(
@@ -336,16 +347,10 @@
     gate_first = jnp.dot(normed, gate_full, preferred_element_type=jnp.float32)
     up_first = jnp.dot(normed, up_full, preferred_element_type=jnp.float32)
     hidden = (jax.nn.silu(gate_first) * up_first).astype(jnp.bfloat16)
-    stream_own = lax.dynamic_slice_in_dim(stream, lax.axis_index("tp") * own_rows, own_rows, 0)
-    stream_own = stream_own + 0.5 * rms_scale(reduce_rows(hidden, down_full), norm_gains[1])
-    normed = rms_scale(stream_own, norm_gains[2]).astype(jnp.bfloat16)
-
-    def project_pool(part_rows, offset):
-        return jnp.dot(part_rows, mix_in_full, preferred_element_type=jnp.float32).astype(
-            jnp.bfloat16
-        )
-
-    pooled_in = gather_rows(normed, project_pool)
+    stream = stream + 0.5 * rms_scale(total_over_tp(hidden, down_full), norm_gains[1])
+    normed = rms_scale(stream, norm_gains[2]).astype(jnp.bfloat16)
+    pooled_in = jnp.dot(normed, mix_in_full, preferred_element_type=jnp.float32)
+    pooled_in = pooled_in.astype(jnp.bfloat16)
     groups_here = pool_w.shape[0]
     group_dim = pool_w.shape[1]
     values = pooled_in.astype(jnp.float32).reshape(rows_all // LEN, LEN, groups_here, group_dim)
@@ -363,16 +368,13 @@
     regrouped = (
         regrouped.reshape(rows_all, groups_here * group_dim) * pool_scale.astype(jnp.float32)
     ).astype(jnp.bfloat16)
-    stream_own = stream_own + rms_scale(reduce_rows(regrouped, mix_out_full), norm_gains[3])
-    normed = rms_scale(stream_own, norm_gains[4]).astype(jnp.bfloat16)
-
-    def project_ffn(part_rows, offset):
-        gate_part = jnp.dot(part_rows, gate_full, preferred_element_type=jnp.float32)
-        up_part = jnp.dot(part_rows, up_full, preferred_element_type=jnp.float32)
-        return (jax.nn.silu(gate_part) * up_part).astype(jnp.bfloat16)
-
-    hidden = gather_rows(normed, project_ffn)
-    stream_own = stream_own + 0.5 * rms_scale(reduce_rows(hidden, down_full), norm_gains[5])
+    stream = stream + rms_scale(total_over_tp(regrouped, mix_out_full), norm_gains[3])
+    normed = rms_scale(stream, norm_gains[4]).astype(jnp.bfloat16)
+    gate_second = jnp.dot(normed, gate_full, preferred_element_type=jnp.float32)
+    up_second = jnp.dot(normed, up_full, preferred_element_type=jnp.float32)
+    hidden = (jax.nn.silu(gate_second) * up_second).astype(jnp.bfloat16)
+    stream_own = own_rows_of(stream)
+    stream_own = stream_own + 0.5 * rms_scale(own_total_over_tp(hidden, down_full), norm_gains[5])
     return stream_own.astype(jnp.bfloat16)
 
 

time: 462 us -> 410 us (0.89)
  waiting for transfers between devices: 48.8 us -> 8.46 us
  between operations: 13.3 us -> 0.17 us
    reduce_scatter x3 -> x0, waiting for transfers between devices: 27.2 us -> none  [reduce_rows(): lax.psum_scatter(jnp.dot(left_rows, right_matrix, preferred_element_type=...]
    all_gather x2 -> x0, waiting for transfers between devices: 21.5 us -> none  [gather_rows(): lax.all_gather(normed, 'tp', axis=0, tiled=True)]
    ppermute x0 -> x3, waiting for transfers between devices: none -> 8.46 us  [the longest x2 6.3 us: total_over_tp(): other = lax.ppermute(part, 'tp', ((0, 1), (1, 0)))]
  transfers between devices with their start and end apart: 5 -> 3, of which waited for: 5 -> 3; matrix products, arithmetic and copies ran while one was open for 0% -> 0% of each run, Pallas kernels for 0% -> 0%
where the time goes in v2:
time: 410 us
  Pallas kernels  319 us (78%)
  matrix products  57.6 us (14%)
  other arithmetic  17.5 us (4%)
  waiting for transfers between devices  8.46 us (2%)
  local copies, waits for them, and re-layouts  6.51 us (2%)
    pallas_call x1, Pallas kernels, gather_weights(): pl.pallas_call(functools.partial(gather_kernel, dims, block, blocks), out...  319 us
    dot_general x2, matrix products, total_over_tp(): part = jnp.dot(left_rows, right_matrix, preferred_element_type=jnp.float32)  18.3 us
    dot_general x1, matrix products, own_total_over_tp(): part = jnp.dot(left_rows, right_matrix, preferred_element_type=jnp.float32)  18.2 us
    reduce_sum x6, other arithmetic, rms_scale(): jnp.mean(values * values, axis=-1, keepdims=True) + 1e-06  13.2 us
    dot_general x1, matrix products, body(): gate_first = jnp.dot(normed, gate_full, preferred_element_type=jnp.float32)  8.76 us
    dot_general x1, matrix products, body(): gate_second = jnp.dot(normed, gate_full, preferred_element_type=jnp.float32)  8.73 us
  transfers between devices with their start and end apart: 3, of which 3 were waited for; matrix products, arithmetic and copies ran while one was open for 0% of the time, Pallas kernels for 0%

profile of v2, /device:TPU:0, one launch (start us, length us, event | category | flops | bytes accessed | tf_op | source)
XLA Modules:
  0.0 409.9 jit_solution(12622547222619645058)
XLA Ops:
  0.0 0.0 copy-start
  0.0 0.0 copy-start.1
  0.0 1.2 fusion.30
  1.2 1.7 fusion.2
  2.8 319.3 %gather_weights.1 = (bf16[2048,2816]{1,0:T(8,128)(2,1)}, bf16[2048,2816]{1,0:T(8,128)(2,1)}, bf16[2816,2048]{1,0:T(8,128)(2,1)}, bf16[2048,512]{1,0:T(8,128)(2,1)}, bf16[512,2048]{1,0:T(8,128)(2,1)}) custom-call(bf16[128,2816]{1,0:T(8,128)(2,1)} %args_0_.4, bf16[128,2816]{1,0:T(8,128)(2,1)} %args_1_.4, bf16[2816,128]{1,0:T(8,128)(2,1)} %args_2_.4, ...), custom_call_target="tpu_custom_call" | custom-call | tf_op jit(solution)/shard_map/gather_weights/pallas_call | solution.py:288
  322.1 0.0 copy-done.1
  322.2 8.8 %fusion.20 = f32[320,2816]{1,0:T(8,128)} fusion(bf16[2048,2816]{1,0:T(8,128)(2,1)} %get-tuple-element.10, bf16[320,2048]{1,0:T(8,128)(2,1)S(1)} %copy-done.1, f32[2048]{0:T(1024)S(1)} %bitcast.38, f32[320]{0:T(512)S(1)} %add_rsqrt_fusion.4), kind=kOutput, calls=%fused_computation.47 | convolution fusion | flops 3693608960 | bytes 16459008 | tf_op jit(solution)/shard_map/dot_general | solution.py:347
  330.9 0.0 copy-start.4
  330.9 16.4 %convolution_convert_fusion.2 = bf16[320,2048]{1,0:T(8,128)(2,1)S(1)} fusion(bf16[2816,2048]{1,0:T(8,128)(2,1)} %get-tuple-element.12, bf16[2048,2816]{1,0:T(8,128)(2,1)} %get-tuple-element.11, f32[320,2816]{1,0:T(8,128)} %fusion.20, bf16[320,2048]{1,0:T(8,128)(2,1)S(1)} %copy-done.1, f32[2048]{0:T(1024)S(1)} %bitcast.39, f32[320]{0:T(512)S(1)} %add_rsqrt_fusion.4), kind=kOutput, calls=%fused_computation.9 | convolution fusion | flops 7390658560 | bytes 29304064 | tf_op jit(solution)/shard_map/dot_general | solution.py:315
  347.4 0.1 collective-permute-start
  347.4 0.0 copy-done.4
  347.5 3.1 collective-permute-done
  350.6 1.8 multiply_reduce_fusion.3
  352.4 0.0 copy-start.6
  352.4 2.5 multiply_reduce_fusion.2
  354.9 0.0 copy-done.6
  354.9 3.3 fusion.9
  358.3 1.3 reshape.106
  359.6 0.0 copy-start.5
  359.6 0.1 fusion.31
  359.7 1.8 fusion.17
  361.5 0.0 copy-done
  361.5 0.2 convolution_bitcast_fusion
  361.8 0.4 copy.12
  362.2 0.0 copy-done.5
  362.2 1.9 convolution_convert_fusion
  364.1 0.1 collective-permute-start.1
  364.3 3.2 collective-permute-done.1
  367.5 2.2 multiply_reduce_fusion.1
  369.7 3.6 multiply_reduce_fusion
  373.3 0.0 copy-start.2
  373.4 1.5 copy-done.2
  374.8 8.7 %fusion.29 = f32[320,2816]{1,0:T(8,128)} fusion(bf16[2048,2816]{1,0:T(8,128)(2,1)} %get-tuple-element.10, f32[320,2048]{1,0:T(8,128)S(1)} %get-tuple-element.16, f32[2048]{0:T(1024)S(1)} %bitcast.35, f32[320]{0:T(512)S(1)} %add_rsqrt_fusion), kind=kOutput, calls=%fused_computation.73 | convolution fusion | flops 3692953600 | bytes 17769728 | tf_op jit(solution)/shard_map/dot_general | solution.py:373
  383.6 18.2 %convolution_convert_fusion.1 = bf16[320,2048]{1,0:T(8,128)(2,1)} fusion(bf16[2816,2048]{1,0:T(8,128)(2,1)} %get-tuple-element.12, bf16[2048,2816]{1,0:T(8,128)(2,1)} %get-tuple-element.11, f32[320,2816]{1,0:T(8,128)} %fusion.29, f32[320,2048]{1,0:T(8,128)} %copy-done.2, f32[2048]{0:T(1024)S(1)} %bitcast.36, f32[320]{0:T(512)S(1)} %add_rsqrt_fusion), kind=kOutput, calls=%fused_computation.8 | convolution fusion | flops 7390003200 | bytes 30614784 | tf_op jit(solution)/shard_map/dot_general | solution.py:324
  401.7 0.0 copy-start.3
  401.7 2.1 constant_dynamic-slice_fusion
  403.9 0.1 collective-permute-start.2
  404.0 2.2 collective-permute-done.2
  406.2 1.4 multiply_reduce_fusion.4
  407.6 0.0 copy-done.3
  407.6 2.3 add_convert_fusion
  (11 shorter events, 0.1 us)
Async XLA Ops:
  0.0 361.5 %copy-start = (bf16[4,128,128]{2,1,0:T(8,128)(2,1)S(1)}, bf16[4,128,128]{2,1,0:T(8,128)(2,1)}, u32[]{:S(2)}) copy-start(bf16[4,128,128]{2,1,0:T(8,128)(2,1)} %param.15) | copy-start | bytes 393220
  0.0 322.1 %copy-start.1 = (bf16[320,2048]{1,0:T(8,128)(2,1)S(1)}, bf16[320,2048]{1,0:T(8,128)(2,1)}, u32[]{:S(2)}) copy-start(bf16[320,2048]{1,0:T(8,128)(2,1)} %param.9) | copy-start | bytes 3932164
  330.9 16.5 %copy-start.4 = (bf16[512]{0:T(512)(128)(2,1)S(1)}, bf16[512]{0:T(512)(128)(2,1)}, u32[]{:S(2)}) copy-start(bf16[512]{0:T(512)(128)(2,1)} %param.16) | copy-start | bytes 3076
  347.4 3.2 collective-permute-start
  352.4 2.5 copy-start.6
  359.6 2.6 copy-start.5
  364.1 3.4 collective-permute-start.1
  373.3 1.5 copy-start.2
  401.7 5.8 %copy-start.3 = (f32[320,2048]{1,0:T(8,128)S(1)}, f32[320,2048]{1,0:T(8,128)}, u32[]{:S(2)}) copy-start(f32[320,2048]{1,0:T(8,128)} %copy-done.2) | copy-start | bytes 7864324
  403.9 2.3 collective-permute-start.2

commit v3 on v2

--- a/solution.py
+++ b/solution.py
@@ -141,43 +141,31 @@
     return max(unit, min(extent - unit, round(extent * share / unit) * unit))
 
 
-def gather_plan(dims, refs, outs, block, blocks):
+def gather_plan(dims, refs, outs, blocks):
     gate, up, down, mix_in, mix_out = refs
     gate_o, up_o, down_o, mix_in_o, mix_out_o = outs
     n = len(dims)
     first = tuple(range(n))
     second = first[1:] + first[:1]
     third = first[-1:] + first[:-1]
-    depth, width = gate.shape
-    across = down.shape[1]
-    mixed = mix_in.shape[1]
     pooled = mix_out.shape[0]
 
-    def columns(ref, out, start_of, size):
+    def rows(ref, out, start_of, size):
         return (
-            lambda c: ref.at[:, pl.ds(start_of(c), size)],
-            lambda c, s: out.at[pl.ds(s * depth, depth), pl.ds(start_of(c), size)],
+            lambda c: ref.at[pl.ds(start_of(c), size), :],
+            lambda c, s: out.at[s, pl.ds(start_of(c), size), :],
         )
 
-    def rows(ref, out, start_of, size):
-        def dst(c, s):
-            if len(out.shape) == 3:
-                return out.at[s, pl.ds(start_of(c), size), :]
-            return out.at[pl.ds(start_of(c), size), pl.ds(s * across, across)]
-
-        return (lambda c: ref.at[pl.ds(start_of(c), size), :], dst)
-
-    def at(offset):
-        if blocks == 1:
-            return lambda c: offset
-        return lambda c: pl.multiple_of(c * block + offset, 16 if offset else block)
-
-    down_cut = cut(block, 16, 2 / 3)
+    def at(block, offset):
+        return lambda c: pl.multiple_of(c * block + offset, 16)
+
+    block, tall = gate.shape[0] // blocks, down.shape[0] // blocks
+    down_cut = cut(tall, 16, 2 / 3)
     main = [
-        Piece(0, dims, first, *columns(gate, gate_o, at(0), block)),
-        Piece(1, dims, third, *columns(up, up_o, at(0), block)),
-        Piece(2, dims, first, *rows(down, down_o, at(0), down_cut)),
-        Piece(3, dims, second, *rows(down, down_o, at(down_cut), block - down_cut)),
+        Piece(0, dims, first, *rows(gate, gate_o, at(block, 0), block)),
+        Piece(1, dims, third, *rows(up, up_o, at(block, 0), block)),
+        Piece(2, dims, first, *rows(down, down_o, at(tall, 0), down_cut)),
+        Piece(3, dims, second, *rows(down, down_o, at(tall, down_cut), tall - down_cut)),
     ]
     mix_cut = cut(pooled, 16, 2 / 3)
 
@@ -185,16 +173,20 @@
         return lambda c: offset
 
     mix = [
-        Piece(0, dims, first, *columns(mix_in, mix_in_o, fixed(0), mixed)),
+        Piece(0, dims, first, *rows(mix_in, mix_in_o, fixed(0), mix_in.shape[0])),
         Piece(1, dims, third, *rows(mix_out, mix_out_o, fixed(0), mix_cut)),
         Piece(2, dims, second, *rows(mix_out, mix_out_o, fixed(mix_cut), pooled - mix_cut)),
     ]
     return main, mix
 
 
-def gather_kernel(dims, block, blocks, *args):
+def gather_kernel(dims, blocks, *args):
     refs, outs = args[:5], args[5:10]
-    send_sem, recv_sem, local_sem = args[10:]
+    beside = None
+    if len(args) > 13:
+        beside = args[10:12]
+        args = args[:10] + args[12:]
+    send_sem, recv_sem, local_sem = args[10:13]
     me = lax.axis_index("fs")
     barrier = pltpu.get_barrier_semaphore()
     expected = 0
@@ -210,7 +202,7 @@
             expected = expected + jnp.where(ok, 1, 0)
     pl.semaphore_wait(barrier, expected)
 
-    main, mix = gather_plan(dims, refs, outs, block, blocks)
+    main, mix = gather_plan(dims, refs, outs, blocks)
     number_sends(main)
     number_sends(mix)
     deepest = sum(size - 1 for size, _ in dims) + 1
@@ -218,19 +210,59 @@
 
     locals_ = []
     for i, (ref, out) in enumerate(zip(refs, outs)):
-        rows_here, columns_here = ref.shape
-        if len(out.shape) == 3:
-            target = out.at[me]
-        elif i in (0, 1, 3):
-            target = out.at[pl.ds(me * rows_here, rows_here), :]
-        else:
-            target = out.at[:, pl.ds(me * columns_here, columns_here)]
-        locals_.append(pltpu.make_async_copy(ref, target, local_sem.at[i]))
+        if beside is not None and i in (2, 4):
+            continue
+        locals_.append(pltpu.make_async_copy(ref, out.at[me], local_sem.at[i]))
 
     go = functools.partial(spread, send_sem=send_sem, recv_sem=recv_sem)
+    def shard_in(source, stage, sem, shard, across):
+        return pltpu.make_async_copy(
+            source, stage.at[:, pl.ds(shard * across, across)], sem.at[shard]
+        )
+
+    def lay_in(own, part, stage, sem, rows, height):
+        for shard in range(part.shape[0]):
+            for mine, source in ((True, own), (False, part.at[shard])):
+
+                @pl.when((me == shard) if mine else (me != shard))
+                def _(source=source, shard=shard):
+                    piece = source.at[pl.ds(rows, height), :]
+                    shard_in(piece, stage, sem, shard, part.shape[2]).start()
+
+    def lay_out(part, whole, stage, sem, rows, height, mode):
+        if mode == "start":
+            for shard in range(part.shape[0]):
+                piece = part.at[shard, pl.ds(rows, height), :]
+                shard_in(piece, stage, sem, shard, part.shape[2]).wait()
+        copy = pltpu.make_async_copy(
+            stage, whole.at[pl.ds(rows, height), :], sem.at[part.shape[0]]
+        )
+        copy.start() if mode == "start" else copy.wait()
+
+    if beside is not None:
+        down_stage, mix_stage, down_sem, mix_sem = args[13:]
+        tall = down_stage.shape[1]
+
+        pooled = mix_stage.shape[0]
+
+    def rows_of(c):
+        return c * tall if isinstance(c, int) else pl.multiple_of(c * tall, 16)
+
+    def down_in(c):
+        slot = c % 2
+        lay_in(refs[2], outs[2], down_stage.at[slot], down_sem.at[slot], rows_of(c), tall)
+
+    def down_out(c, mode="start"):
+        slot = c % 2
+        lay_out(outs[2], beside[0], down_stage.at[slot], down_sem.at[slot], rows_of(c), tall, mode)
+
+    go(mix, me, blocks, low=0, high=1, mode="start")
     go(main, me, 0, low=0, high=1, mode="start")
     for copy in locals_:
         copy.start()
+    go(mix, me, blocks, low=1, high=deepest, mode="start")
+    if beside is not None:
+        lay_in(refs[4], outs[4], mix_stage, mix_sem, 0, pooled)
 
     def step(i, carry):
         @pl.when(i + 1 < blocks)
@@ -243,12 +275,32 @@
         def _():
             go(main, me, i - 1, low=early, high=deepest, mode="start")
 
+        if beside is not None:
+
+            @pl.when(i > 2)
+            def _():
+                down_out(i - 3, "end")
+
+            @pl.when(i > 0)
+            def _():
+                down_in(i - 1)
+
+            @pl.when(i > 1)
+            def _():
+                down_out(i - 2)
+
         return carry
 
     lax.fori_loop(0, blocks, step, 0)
-    go(mix, me, blocks, low=0, high=1, mode="start")
     go(main, me, blocks - 1, low=early, high=deepest, mode="start")
-    go(mix, me, blocks, low=1, high=deepest, mode="start")
+    if beside is not None:
+        if blocks > 2:
+            down_out(blocks - 3, "end")
+        down_in(blocks - 1)
+        if blocks > 1:
+            down_out(blocks - 2)
+        lay_out(outs[4], beside[1], mix_stage, mix_sem, 0, pooled, "start")
+        down_out(blocks - 1)
 
     def finish(i, carry):
         go(main, me, i, low=0, high=deepest, mode="end")
@@ -256,6 +308,11 @@
 
     lax.fori_loop(0, blocks, finish, 0)
     go(mix, me, blocks, low=0, high=deepest, mode="end")
+    if beside is not None:
+        if blocks > 1:
+            down_out(blocks - 2, "end")
+        down_out(blocks - 1, "end")
+        lay_out(outs[4], beside[1], mix_stage, mix_sem, 0, pooled, "end")
     for copy in locals_:
         copy.wait()
 
@@ -264,47 +321,53 @@
     count = 1
     for size, _ in dims:
         count *= size
-    width = w_gate.shape[1]
-    block = next((b for b in (256, 128) if width % b == 0), width)
-    blocks = width // block
-
-    def rows_out(a):
-        return jax.ShapeDtypeStruct((a.shape[0] * count, a.shape[1]), a.dtype)
-
-    def columns_out(a):
-        if a.shape[1] % 128 == 0:
-            return jax.ShapeDtypeStruct((a.shape[0], a.shape[1] * count), a.dtype)
-        return jax.ShapeDtypeStruct((count, *a.shape), a.dtype)
-
-    shapes = [rows_out(w_gate), rows_out(w_up), columns_out(w_down)]
-    shapes += [rows_out(w_mix_in), columns_out(w_mix_out)]
+    tiles = (w_gate.shape[0] // 16, w_down.shape[0] // 16)
+    blocks = next(b for b in (8, 4, 2, 1) if tiles[0] % b == 0 and tiles[1] % b == 0)
+    weights = (w_gate, w_up, w_down, w_mix_in, w_mix_out)
+    shapes = [jax.ShapeDtypeStruct((count, *a.shape), a.dtype) for a in weights]
+
     class Shape:
         def __init__(self, shape):
             self.shape = shape
 
-    stand_in = [Shape(a.shape) for a in (w_gate, w_up, w_down, w_mix_in, w_mix_out)]
-    main, mix = gather_plan(dims, stand_in, [Shape(s.shape) for s in shapes], block, blocks)
+    stand_in = [Shape(a.shape) for a in weights]
+    main, mix = gather_plan(dims, stand_in, [Shape(s.shape) for s in shapes], blocks)
     sends = max(number_sends(main), number_sends(mix))
+    scratch = [
+        pltpu.SemaphoreType.DMA((blocks + 1, sends)),
+        pltpu.SemaphoreType.DMA((blocks + 1, len(main), count)),
+        pltpu.SemaphoreType.DMA((5,)),
+    ]
+    laid = w_down.shape[1] % 128 == 0
+    if laid:
+        tall, full = w_down.shape[0] // blocks, w_down.shape[1] * count
+        shapes += [jax.ShapeDtypeStruct((a.shape[0], full), a.dtype) for a in (w_down, w_mix_out)]
+        scratch += [
+            pltpu.VMEM((2, tall, full), w_down.dtype),
+            pltpu.VMEM((w_mix_out.shape[0], full), w_mix_out.dtype),
+            pltpu.SemaphoreType.DMA((2, count + 1)),
+            pltpu.SemaphoreType.DMA((count + 1,)),
+        ]
     outs = pl.pallas_call(
-        functools.partial(gather_kernel, dims, block, blocks),
+        functools.partial(gather_kernel, dims, blocks),
         out_shape=shapes,
         in_specs=[pl.BlockSpec(memory_space=pltpu.HBM)] * 5,
-        out_specs=[pl.BlockSpec(memory_space=pltpu.HBM)] * 5,
-        scratch_shapes=[
-            pltpu.SemaphoreType.DMA((blocks + 1, sends)),
-            pltpu.SemaphoreType.DMA((blocks + 1, len(main), count)),
-            pltpu.SemaphoreType.DMA((5,)),
-        ],
+        out_specs=[pl.BlockSpec(memory_space=pltpu.HBM)] * len(shapes),
+        scratch_shapes=scratch,
         compiler_params=pltpu.CompilerParams(collective_id=0, has_side_effects=True),
         name="gather_weights",
-    )(w_gate, w_up, w_down, w_mix_in, w_mix_out)
-
-    def flat(a):
-        if a.ndim == 2:
-            return a
+    )(*weights)
+
+    def stacked(a):
+        return a.reshape(-1, a.shape[2])
+
+    def beside(a):
         return jnp.transpose(a, (1, 0, 2)).reshape(a.shape[1], -1)
 
-    return [flat(a) for a in outs]
+    gate, up, down, mix_in, mix_out = outs[:5]
+    if laid:
+        return stacked(gate), stacked(up), outs[5], stacked(mix_in), outs[6]
+    return stacked(gate), stacked(up), beside(down), stacked(mix_in), beside(mix_out)
 
 
 def rms_scale(values, gain):

time: 410 us -> 391 us (0.954)
  Pallas kernels: 319 us -> 300 us
    pallas_call x1, Pallas kernels: 319 us -> 300 us  [gather_weights(): pl.pallas_call(functools.partial(gather_kernel, dims, blocks), out_shape=...]
where the time goes in v3:
time: 391 us
  Pallas kernels  300 us (77%)
  matrix products  57.6 us (15%)
  other arithmetic  17.5 us (4%)
  waiting for transfers between devices  8.47 us (2%)
  local copies, waits for them, and re-layouts  6.51 us (2%)
    pallas_call x1, Pallas kernels, gather_weights(): pl.pallas_call(functools.partial(gather_kernel, dims, blocks), out_shape=...  300 us
    dot_general x2, matrix products, total_over_tp(): part = jnp.dot(left_rows, right_matrix, preferred_element_type=jnp.float32)  18.3 us
    dot_general x1, matrix products, own_total_over_tp(): part = jnp.dot(left_rows, right_matrix, preferred_element_type=jnp.float32)  18.2 us
    reduce_sum x6, other arithmetic, rms_scale(): jnp.mean(values * values, axis=-1, keepdims=True) + 1e-06  13.2 us
    dot_general x1, matrix products, body(): gate_first = jnp.dot(normed, gate_full, preferred_element_type=jnp.float32)  8.75 us
    dot_general x1, matrix products, body(): gate_second = jnp.dot(normed, gate_full, preferred_element_type=jnp.float32)  8.72 us
  transfers between devices with their start and end apart: 3, of which 3 were waited for; matrix products, arithmetic and copies ran while one was open for 0% of the time, Pallas kernels for 0%

profile of v3, /device:TPU:0, one launch (start us, length us, event | category | flops | bytes accessed | tf_op | source)
XLA Modules:
  0.0 390.9 jit_solution(15200503720500681430)
XLA Ops:
  0.0 0.0 copy-start
  0.0 0.0 copy-start.2
  0.0 1.2 fusion.30
  1.2 1.7 fusion.2
  2.8 300.4 %gather_weights.1 = (bf16[16,128,2816]{2,1,0:T(8,128)(2,1)}, bf16[16,128,2816]{2,1,0:T(8,128)(2,1)}, bf16[16,2816,128]{2,1,0:T(8,128)(2,1)}, bf16[16,128,512]{2,...) custom-call(bf16[128,2816]{1,0:T(8,128)(2,1)} %args_0_.4, ...), custom_call_target="tpu_custom_call" | custom-call | tf_op jit(solution)/shard_map/gather_weights/pallas_call | solution.py:351
  303.2 0.0 copy-done.2
  303.2 8.8 %fusion.20 = f32[320,2816]{1,0:T(8,128)} fusion(bf16[2048,2816]{1,0:T(8,128)(2,1)} %bitcast.45, bf16[320,2048]{1,0:T(8,128)(2,1)S(1)} %copy-done.2, f32[2048]{0:T(1024)S(1)} %bitcast.41, f32[320]{0:T(512)S(1)} %add_rsqrt_fusion.4), kind=kOutput, calls=%fused_computation.47 | convolution fusion | flops 3693608960 | bytes 16459008 | tf_op jit(solution)/shard_map/dot_general | solution.py:410
  312.0 0.0 copy-start.5
  312.0 16.4 %convolution_convert_fusion.2 = bf16[320,2048]{1,0:T(8,128)(2,1)S(1)} fusion(bf16[2816,2048]{1,0:T(8,128)(2,1)} %get-tuple-element.12, bf16[2048,2816]{1,0:T(8,128)(2,1)} %bitcast.43, f32[320,2816]{1,0:T(8,128)} %fusion.20, bf16[320,2048]{1,0:T(8,128)(2,1)S(1)} %copy-done.2, f32[2048]{0:T(1024)S(1)} %bitcast.42, f32[320]{0:T(512)S(1)} %add_rsqrt_fusion.4), kind=kOutput, calls=%fused_computation.9 | convolution fusion | flops 7390658560 | bytes 29304064 | tf_op jit(solution)/shard_map/dot_general | solution.py:378
  328.4 0.1 collective-permute-start
  328.5 0.0 copy-done.5
  328.6 3.1 collective-permute-done
  331.6 1.8 multiply_reduce_fusion.3
  333.5 0.0 copy-start.7
  333.5 2.4 multiply_reduce_fusion.2
  335.9 0.0 copy-done.7
  335.9 3.3 fusion.9
  339.3 1.3 reshape.118
  340.6 0.0 copy-start.6
  340.6 0.1 fusion.31
  340.7 1.8 fusion.17
  342.5 0.0 copy-done
  342.5 0.2 convolution_bitcast_fusion
  342.8 0.4 copy.12
  343.2 0.0 copy-done.6
  343.2 1.9 convolution_convert_fusion
  345.1 0.1 collective-permute-start.1
  345.3 3.2 collective-permute-done.1
  348.5 2.2 multiply_reduce_fusion.1
  350.8 3.6 multiply_reduce_fusion
  354.4 0.0 copy-start.3
  354.4 1.5 copy-done.3
  355.9 8.7 %fusion.29 = f32[320,2816]{1,0:T(8,128)} fusion(bf16[2048,2816]{1,0:T(8,128)(2,1)} %bitcast.46, f32[320,2048]{1,0:T(8,128)S(1)} %get-tuple-element.16, f32[2048]{0:T(1024)S(1)} %bitcast.38, f32[320]{0:T(512)S(1)} %add_rsqrt_fusion), kind=kOutput, calls=%fused_computation.73 | convolution fusion | flops 3692953600 | bytes 17769728 | tf_op jit(solution)/shard_map/dot_general | solution.py:436
  364.6 18.2 %convolution_convert_fusion.1 = bf16[320,2048]{1,0:T(8,128)(2,1)} fusion(bf16[2816,2048]{1,0:T(8,128)(2,1)} %get-tuple-element.12, bf16[2048,2816]{1,0:T(8,128)(2,1)} %bitcast.44, f32[320,2816]{1,0:T(8,128)} %fusion.29, f32[320,2048]{1,0:T(8,128)} %copy-done.3, f32[2048]{0:T(1024)S(1)} %bitcast.39, f32[320]{0:T(512)S(1)} %add_rsqrt_fusion), kind=kOutput, calls=%fused_computation.8 | convolution fusion | flops 7390003200 | bytes 30614784 | tf_op jit(solution)/shard_map/dot_general | solution.py:387
  382.7 0.0 copy-start.4
  382.7 0.0 copy-start.1
  382.8 2.1 constant_dynamic-slice_fusion
  384.9 0.1 collective-permute-start.2
  385.0 2.2 collective-permute-done.2
  387.2 1.4 multiply_reduce_fusion.4
  388.6 0.0 copy-done.4
  388.6 2.3 add_convert_fusion
  390.9 0.0 copy-done.1
  (11 shorter events, 0.1 us)
Async XLA Ops:
  0.0 342.5 %copy-start = (bf16[4,128,128]{2,1,0:T(8,128)(2,1)S(1)}, bf16[4,128,128]{2,1,0:T(8,128)(2,1)}, u32[]{:S(2)}) copy-start(bf16[4,128,128]{2,1,0:T(8,128)(2,1)} %param.15) | copy-start | bytes 393220
  0.0 303.2 %copy-start.2 = (bf16[320,2048]{1,0:T(8,128)(2,1)S(1)}, bf16[320,2048]{1,0:T(8,128)(2,1)}, u32[]{:S(2)}) copy-start(bf16[320,2048]{1,0:T(8,128)(2,1)} %param.9) | copy-start | bytes 3932164
  312.0 16.5 %copy-start.5 = (bf16[512]{0:T(512)(128)(2,1)S(1)}, bf16[512]{0:T(512)(128)(2,1)}, u32[]{:S(2)}) copy-start(bf16[512]{0:T(512)(128)(2,1)} %param.16) | copy-start | bytes 3076
  328.4 3.2 collective-permute-start
  333.5 2.5 copy-start.7
  340.6 2.6 copy-start.6
  345.1 3.4 collective-permute-start.1
  354.4 1.5 copy-start.3
  382.7 5.8 %copy-start.4 = (f32[320,2048]{1,0:T(8,128)S(1)}, f32[320,2048]{1,0:T(8,128)}, u32[]{:S(2)}) copy-start(f32[320,2048]{1,0:T(8,128)} %copy-done.3) | copy-start | bytes 7864324
  382.7 8.2 %copy-start.1 = (bf16[4,128,128]{2,1,0:T(8,128)(2,1)S(1)}, bf16[4,128,128]{2,1,0:T(8,128)(2,1)}, u32[]{:S(2)}) copy-start(bf16[4,128,128]{2,1,0:T(8,128)(2,1)} %param.15) | copy-start | bytes 393220
  384.9 2.3 collective-permute-start.2
